TPU v7x, 32 devices: a whole 2x2x4 slice. The times are simulated.
32 devices in a mesh: sp: 4 (over z), tp: 4 (over y, x), dp: 2 (over core).
Axes of the slice: x: 2, y: 2, z: 4, core: 2. Of those that a mesh axis runs over, the one named last changes fastest.
Arguments:
- latent_in: bfloat16 [3072, 2048], P(('dp', 'sp', 'tp')), parts along dimension 0, may hold values from -6 to 6
- condition: bfloat16 [4096], P(('dp', 'sp')), parts along dimension 0, may hold values from -8 to 8
- context_latent: bfloat16 [1024, 256], P(('dp', 'sp')), parts along dimension 0, may hold values from -6 to 6
- context_rope: bfloat16 [1024, 64], P(('dp', 'sp')), parts along dimension 0, may hold values from -6 to 6
- shift_weight: bfloat16 [2048, 2048], P('sp', 'tp'), may hold values from -0.125 to 0.125
- scale_weight: bfloat16 [2048, 2048], P('sp', 'tp'), may hold values from -0.125 to 0.125
- gate_weight: bfloat16 [2048, 2048], P('sp', 'tp'), may hold values from -0.125 to 0.125
- norm_gain: float32 [2048], replicated, may hold values from 0.1 to 1.9
- down_query: bfloat16 [2048, 512], replicated, may hold values from -0.125 to 0.125
- down_latent: bfloat16 [2048, 256], replicated, may hold values from -0.125 to 0.125
- down_rope: bfloat16 [2048, 64], replicated, may hold values from -0.125 to 0.125
- query_gain: float32 [512], replicated, may hold values from 0.5 to 60
- latent_gain: float32 [256], replicated, may hold values from 0.1 to 1.9
- up_query: bfloat16 [512, 1536], P(None, 'tp'), may hold values from -0.25 to 0.25
- up_key: bfloat16 [256, 1024], P(None, 'tp'), may hold values from -0.375 to 0.375
- up_value: bfloat16 [256, 1024], P(None, 'tp'), may hold values from -0.375 to 0.375
- context_bias: float32 [8], P('tp'), may hold values from 1 to 2.5
- out_weight: bfloat16 [1024, 2048], replicated, may hold values from -3 to 3
Outputs:
- mixed_out: bfloat16 [3072, 2048], P(('dp', 'sp', 'tp')), parts along dimension 0
There are 2 independent parts, one for each index of `dp`. A program takes and returns all parts, laid end to end along the dimension named above; an argument that names none is the same for every part. Nothing has to cross between parts.
All inputs are finite; a program needn't handle non-finite values.
Results may differ from a plain program's by a relative error of at most 0.039.
The roundings to bfloat16 on the way count: a program that leaves them out, or rounds other values in their place, can miss the bound.
Values may be sent and summed in bfloat16 or wider, within the bound.
A program may use at most 128 MiB of HBM per device.

v0:
```python
import jax
import jax.numpy as jnp
from jax import lax
from jax.sharding import PartitionSpec as P

QK_NOPE = 128
QK_ROPE = 64
V_HEAD = 128
GRID_W = 64
epsilon = 1e-06
rope_base = 10000.0
block_limit = 2048


def rms_scaled(values, gain_vec):
    mean_sq = jnp.mean(values * values, axis=-1, keepdims=True)
    return values * lax.rsqrt(mean_sq + epsilon) * gain_vec


def rope_tables(positions, rope_width):
    freq_count = rope_width // 4
    inverse = rope_base ** (-jnp.arange(freq_count, dtype=jnp.float32) / freq_count)
    grid_row = (positions // GRID_W).astype(jnp.float32)
    grid_col = (positions % GRID_W).astype(jnp.float32)
    row_angle = grid_row[:, None] * inverse
    col_angle = grid_col[:, None] * inverse
    angles = jnp.concatenate([row_angle, row_angle, col_angle, col_angle], axis=-1)
    return (jnp.cos(angles), jnp.sin(angles))


def rope_turn(values, cosine_table, sine_table):
    part_one, part_two, part_three, part_four = jnp.split(values, 4, axis=-1)
    turned = jnp.concatenate([-part_two, part_one, -part_four, part_three], axis=-1)
    return values * cosine_table + turned * sine_table


def attend(attn_state, query_nope, query_rope, keys_nope, values_in, keys_rope, bias_col):
    score_scale = (query_nope.shape[-1] + query_rope.shape[-1]) ** (-0.5)
    scores = jnp.einsum("thd,khd->htk", query_nope, keys_nope, preferred_element_type=jnp.float32)
    scores = scores + jnp.einsum(
        "thr,kr->htk", query_rope, keys_rope, preferred_element_type=jnp.float32
    )
    scores = scores * score_scale + bias_col
    run_max, run_total, run_acc = attn_state
    new_max = jnp.maximum(run_max, jnp.max(scores, axis=-1))
    shrink = jnp.exp(run_max - new_max)
    weights = jnp.exp(scores - new_max[:, :, None])
    new_total = run_total * shrink + jnp.sum(weights, axis=-1)
    new_acc = run_acc * shrink[:, :, None] + jnp.einsum(
        "htk,khd->htd", weights.astype(jnp.bfloat16), values_in, preferred_element_type=jnp.float32
    )
    return (new_max, new_total, new_acc)


def over_blocks(attn_state, arrays, handle):
    row_count = arrays[0].shape[0]
    block_rows = 1
    for candidate in range(min(row_count, block_limit), 0, -1):
        if row_count % candidate == 0:
            block_rows = candidate
            break
    block_count = row_count // block_rows
    if block_count == 1:
        return handle(attn_state, arrays)
    stacked = tuple(
        (array_in.reshape((block_count, block_rows) + array_in.shape[1:]) for array_in in arrays)
    )

    def one_turn(inner_state, pieces):
        return (handle(inner_state, pieces), None)

    return lax.scan(one_turn, attn_state, stacked)[0]


def on_device(
    latent_in,
    condition,
    context_latent,
    context_rope,
    shift_weight,
    scale_weight,
    gate_weight,
    norm_gain,
    down_query,
    down_latent,
    down_rope,
    query_gain,
    latent_gain,
    up_query,
    up_key,
    up_value,
    context_bias,
    out_weight,
):
    activated = jax.nn.silu(condition.astype(jnp.float32)).astype(jnp.bfloat16)
    partials = jnp.stack(
        [
            jnp.dot(activated, weight_in, preferred_element_type=jnp.float32)
            for weight_in in (shift_weight, scale_weight, gate_weight)
        ]
    )
    summed = lax.psum(partials, "sp")
    modulation = lax.all_gather(summed, "tp", axis=1, tiled=True)
    shift_vec = modulation[0]
    scale_vec = modulation[1]
    gate_vec = modulation[2]
    residual_in = latent_in.astype(jnp.float32)
    normed = (rms_scaled(residual_in, norm_gain) * (1.0 + scale_vec) + shift_vec).astype(
        jnp.bfloat16
    )
    query_low = rms_scaled(
        jnp.dot(normed, down_query, preferred_element_type=jnp.float32), query_gain
    ).astype(jnp.bfloat16)
    latent_low = rms_scaled(
        jnp.dot(normed, down_latent, preferred_element_type=jnp.float32), latent_gain
    ).astype(jnp.bfloat16)
    local_rows = latent_in.shape[0]
    first_row = (lax.axis_index("sp") * lax.axis_size("tp") + lax.axis_index("tp")) * local_rows
    own_positions = first_row + jnp.arange(local_rows, dtype=jnp.int32)
    own_cosine, own_sine = rope_tables(own_positions, QK_ROPE)
    rope_keys = rope_turn(
        jnp.dot(normed, down_rope, preferred_element_type=jnp.float32), own_cosine, own_sine
    ).astype(jnp.bfloat16)
    query_group, latent_group, rope_group = (
        lax.all_gather(query_low, "tp", axis=0, tiled=True),
        lax.all_gather(latent_low, "tp", axis=0, tiled=True),
        lax.all_gather(rope_keys, "tp", axis=0, tiled=True),
    )
    group_rows = query_group.shape[0]
    group_positions = lax.axis_index("sp") * group_rows + jnp.arange(group_rows, dtype=jnp.int32)
    group_cosine, group_sine = rope_tables(group_positions, QK_ROPE)
    head_count = up_key.shape[1] // QK_NOPE
    queries = jnp.dot(query_group, up_query, preferred_element_type=jnp.float32).reshape(
        group_rows, head_count, QK_NOPE + QK_ROPE
    )
    query_nope = queries[:, :, :QK_NOPE].astype(jnp.bfloat16)
    query_rope = rope_turn(
        queries[:, :, QK_NOPE:], group_cosine[:, None, :], group_sine[:, None, :]
    ).astype(jnp.bfloat16)
    context_all, context_keys_rope = (
        lax.all_gather(context_latent, "sp", axis=0, tiled=True),
        lax.all_gather(context_rope, "sp", axis=0, tiled=True),
    )
    context_count = context_all.shape[0]
    context_nope = (
        jnp.dot(context_all, up_key, preferred_element_type=jnp.float32)
        .astype(jnp.bfloat16)
        .reshape(context_count, head_count, QK_NOPE)
    )
    context_values = (
        jnp.dot(context_all, up_value, preferred_element_type=jnp.float32)
        .astype(jnp.bfloat16)
        .reshape(context_count, head_count, V_HEAD)
    )
    start_state = (
        jnp.full((head_count, group_rows), -jnp.inf, jnp.float32),
        jnp.zeros((head_count, group_rows), jnp.float32),
        jnp.zeros((head_count, group_rows, V_HEAD), jnp.float32),
    )
    bias_col = context_bias[:, None, None]

    def context_step(inner_state, pieces):
        return attend(
            inner_state, query_nope, query_rope, pieces[0], pieces[1], pieces[2], bias_col
        )

    attn_state = over_blocks(
        start_state, (context_nope, context_values, context_keys_rope), context_step
    )
    own_nope = jnp.dot(latent_group, up_key, preferred_element_type=jnp.float32).astype(
        jnp.bfloat16
    )
    own_values = jnp.dot(latent_group, up_value, preferred_element_type=jnp.float32).astype(
        jnp.bfloat16
    )

    def expanded_step(inner_state, pieces):
        piece_rows = pieces[0].shape[0]
        return attend(
            inner_state,
            query_nope,
            query_rope,
            pieces[0].reshape(piece_rows, head_count, QK_NOPE),
            pieces[1].reshape(piece_rows, head_count, V_HEAD),
            pieces[2],
            0.0,
        )

    attn_state = over_blocks(
        attn_state,
        (
            lax.all_gather(own_nope, "sp", axis=0, tiled=True),
            lax.all_gather(own_values, "sp", axis=0, tiled=True),
            lax.all_gather(rope_group, "sp", axis=0, tiled=True),
        ),
        expanded_step,
    )
    attended = (attn_state[2] / attn_state[1][:, :, None]).astype(jnp.bfloat16)
    attended = attended.transpose(1, 0, 2).reshape(group_rows, head_count * V_HEAD)
    token_major = lax.all_to_all(attended, "tp", split_axis=0, concat_axis=1, tiled=True)
    mixed = jnp.dot(token_major, out_weight, preferred_element_type=jnp.float32)
    return (residual_in + gate_vec * mixed).astype(jnp.bfloat16)


def solution(mesh):
    in_specs = (
        P(("dp", "sp", "tp"), None),
        P(("dp", "sp")),
        P(("dp", "sp"), None),
        P(("dp", "sp"), None),
        P("sp", "tp"),
        P("sp", "tp"),
        P("sp", "tp"),
        P(),
        P(),
        P(),
        P(),
        P(),
        P(),
        P(None, "tp"),
        P(None, "tp"),
        P(None, "tp"),
        P("tp"),
        P(),
    )
    out_specs = P(("dp", "sp", "tp"), None)
    return jax.shard_map(
        on_device, mesh=mesh, in_specs=in_specs, out_specs=out_specs, check_vma=False
    )
```

profile of v0, /device:TPU:0, one launch (start us, length us, event | category | flops | bytes accessed | tf_op | source)
XLA Modules:
  0.0 158.6 jit_solution(2897633564219635338)
XLA Ops:
  0.6 0.7 fusion.54
  1.3 1.2 fusion.72
  2.6 1.2 fusion.73
  3.8 1.3 fusion.74
  5.1 13.8 %psum.7 = f32[3,512]{1,0:T(4,128)S(1)} all-reduce(f32[3,512]{1,0:T(4,128)S(1)} %pad_maximum_fusion.2), channel_id=1, replica_groups=mesh['sp'=4,'tp'=4,'dp'=2] {'sp'}, use_global_device_ids=true, to_apply=%region_0.1 | all-reduce | flops 1536 | bytes 12288 | tf_op jit(solution)/shard_map/psum | solution.py:102
  18.9 8.2 %all_gather.27 = f32[3,2048]{1,0:T(4,128)S(1)} all-gather(f32[3,512]{1,0:T(4,128)S(1)} %psum.7), channel_id=1, replica_groups=mesh['sp'=4,'tp'=4,'dp'=2] {'tp'}, dimensions={1}, use_global_device_ids=true | all-gather | bytes 30720 | tf_op jit(solution)/shard_map/all_gather | solution.py:103
  27.1 1.2 fusion.26
  28.4 1.9 %multiply_reduce_fusion.1 = (f32[96]{0:T(128)S(1)}, f32[96,256]{1,0:T(8,128)S(1)}) fusion(bf16[2048,256]{1,0:T(8,128)(2,1)} %param.27, bf16[96,2048]{1,0:T(8,128)(2,1)} %param.18, f32[2048]{0:T(1024)S(1)} %bitcast.119, f32[2048]{0:T(1024)S(1)} %bitcast.122, f32[2048]{0:T(1024)} %param.25, f32[96]{0:T(128)S(1)} %add_rsqrt_fusion.2), kind=kOutput, calls=%fused_computation.50 | convolution fusion | flops 101892000 | bytes 1565440 | tf_op jit(solution)/shard_map/dot_general | solution.py:115
  30.3 8.7 %all_gather.31 = bf16[384,256]{1,0:T(8,128)(2,1)S(1)} all-gather(bf16[96,256]{1,0:T(8,128)(2,1)S(1)} %multiply_convert_fusion.1), channel_id=1, replica_groups=mesh['sp'=4,'tp'=4,'dp'=2] {'tp'}, dimensions={0}, use_global_device_ids=true | all-gather | bytes 245760 | tf_op jit(solution)/shard_map/all_gather | solution.py:126
  39.1 13.8 %all_gather.29 = bf16[512,256]{1,0:T(8,128)(2,1)S(1)} all-gather(bf16[128,256]{1,0:T(8,128)(2,1)S(1)} %copy-done.12), channel_id=1, replica_groups=mesh['sp'=4,'tp'=4,'dp'=2] {'sp'}, dimensions={0}, use_global_device_ids=true | all-gather | bytes 327680 | tf_op jit(solution)/shard_map/all_gather | solution.py:141
  52.9 0.9 convolution_convert_fusion.3
  54.0 1.0 convolution_convert_fusion
  56.0 8.5 %all_gather.28 = bf16[384,512]{1,0:T(8,128)(2,1)S(1)} all-gather(bf16[96,512]{1,0:T(8,128)(2,1)S(1)} %multiply_convert_fusion), channel_id=1, replica_groups=mesh['sp'=4,'tp'=4,'dp'=2] {'tp'}, dimensions={0}, use_global_device_ids=true | all-gather | bytes 491520 | tf_op jit(solution)/shard_map/all_gather | solution.py:125
  65.0 0.7 slice_negate_fusion.1
  66.3 1.3 fusion.62
  67.6 0.6 copy-done.11
  68.9 0.7 broadcast_multiply_fusion.3
  69.6 0.9 fusion.47
  70.5 8.2 %all-gather = bf16[4,96,64]{1,2,0:T(8,128)(2,1)S(1)} all-gather(bf16[1,96,64]{1,2,0:T(8,128)(2,1)S(1)} %fusion.47), channel_id=1, replica_groups=mesh['sp'=4,'tp'=4,'dp'=2] {'tp'}, dimensions={0}, use_global_device_ids=true | all-gather | bytes 61440 | tf_op jit(solution)/shard_map/all_gather | solution.py:127
  78.7 0.7 copy.48
  79.4 1.6 reshape.254
  81.0 14.6 %all_gather.34 = bf16[1536,64]{0,1:T(8,128)(2,1)S(1)} all-gather(bf16[384,64]{0,1:T(8,128)(2,1)} %reshape.254), channel_id=1, replica_groups=mesh['sp'=4,'tp'=4,'dp'=2] {'sp'}, dimensions={0}, use_global_device_ids=true | all-gather | bytes 245760 | tf_op jit(solution)/shard_map/all_gather | solution.py:194
  95.6 16.9 %all_gather.32 = bf16[1536,256]{1,0:T(8,128)(2,1)S(1)} all-gather(bf16[384,256]{1,0:T(8,128)(2,1)} %convolution_convert_fusion.3), channel_id=1, replica_groups=mesh['sp'=4,'tp'=4,'dp'=2] {'sp'}, dimensions={0}, use_global_device_ids=true | all-gather | bytes 983040 | tf_op jit(solution)/shard_map/all_gather | solution.py:192
  112.9 12.2 %all_gather.30 = bf16[512,64]{0,1:T(8,128)(2,1)S(1)} all-gather(bf16[128,64]{0,1:T(8,128)(2,1)S(1)} %copy-done.13), channel_id=1, replica_groups=mesh['sp'=4,'tp'=4,'dp'=2] {'sp'}, dimensions={0}, use_global_device_ids=true | all-gather | bytes 81920 | tf_op jit(solution)/shard_map/all_gather | solution.py:142
  125.4 0.8 fusion.39
  126.3 1.0 fusion.71
  128.3 15.6 %all_gather.35 = bf16[1536,256]{1,0:T(8,128)(2,1)S(1)} all-gather(bf16[384,256]{1,0:T(8,128)(2,1)S(1)} %convolution_convert_fusion.2), channel_id=1, replica_groups=mesh['sp'=4,'tp'=4,'dp'=2] {'sp'}, dimensions={0}, use_global_device_ids=true | all-gather | bytes 983040 | tf_op jit(solution)/shard_map/all_gather | solution.py:193
  143.8 0.8 fusion.1
  144.8 0.7 fusion.19
  145.5 0.9 fusion.23
  146.8 8.1 %all_to_all.19 = bf16[4,96,256]{2,1,0:T(8,128)(2,1)S(1)} all-to-all(bf16[4,96,256]{2,1,0:T(8,128)(2,1)S(1)} %all_to_all.14), channel_id=1, replica_groups=mesh['sp'=4,'tp'=4,'dp'=2] {'tp'}, dimensions={0} | all-to-all | bytes 393216 | tf_op jit(solution)/shard_map/all_to_all | solution.py:200
  154.9 3.8 %fusion.7 = bf16[96,2048]{1,0:T(8,128)(2,1)} fusion(bf16[96,1024]{1,0:T(8,128)(2,1)S(1)} %bitcast.116, bf16[1024,2048]{1,0:T(8,128)(2,1)} %param.35, bf16[96,2048]{1,0:T(8,128)(2,1)S(1)} %copy-done.1, f32[2048]{0:T(1024)S(1)} %bitcast.118), kind=kOutput, calls=%fused_computation.9 | convolution fusion | flops 403439616 | bytes 5185536 | tf_op jit(solution)/shard_map/dot_general | solution.py:201
  (72 shorter events, 5.8 us)
Async XLA Ops:
  0.0 55.3 %copy-start = (bf16[2048,512]{1,0:T(8,128)(2,1)S(1)}, bf16[2048,512]{1,0:T(8,128)(2,1)}, u32[]{:S(2)}) copy-start(bf16[2048,512]{1,0:T(8,128)(2,1)} %param.26) | copy-start | bytes 6291460
  0.0 30.2 %copy-start.19 = (f32[256]{0:T(256)S(1)}, f32[256]{0:T(256)}, u32[]{:S(2)}) copy-start(f32[256]{0:T(256)} %param.30) | copy-start | bytes 3076
  0.0 39.0 %copy-start.12 = (bf16[128,256]{1,0:T(8,128)(2,1)S(1)}, bf16[128,256]{1,0:T(8,128)(2,1)}, u32[]{:S(2)}) copy-start(bf16[128,256]{1,0:T(8,128)(2,1)} %param.20) | copy-start | bytes 196612
  1.3 51.5 %copy-start.3 = (bf16[256,256]{1,0:T(8,128)(2,1)S(1)}, bf16[256,256]{1,0:T(8,128)(2,1)}, u32[]{:S(2)}) copy-start(bf16[256,256]{1,0:T(8,128)(2,1)} %param.32) | copy-start | bytes 393220
  3.8 50.2 %copy-start.4 = (bf16[256,256]{1,0:T(8,128)(2,1)S(1)}, bf16[256,256]{1,0:T(8,128)(2,1)}, u32[]{:S(2)}) copy-start(bf16[256,256]{1,0:T(8,128)(2,1)} %param.33) | copy-start | bytes 393220
  27.1 28.1 %copy-start.14 = (f32[1,2048]{1,0:T(1,128)}, f32[1,2048]{1,0:T(1,128)S(1)}, u32[]{:S(2)}) copy-start(f32[1,2048]{1,0:T(1,128)S(1)} %get-tuple-element.15) | copy-start | bytes 24580
  27.1 27.9 %copy-start.5 = (bf16[256,256]{1,0:T(8,128)(2,1)S(1)}, bf16[256,256]{1,0:T(8,128)(2,1)}, u32[]{:S(2)}) copy-start(bf16[256,256]{1,0:T(8,128)(2,1)} %param.33) | copy-start | bytes 393220
  28.3 26.9 %copy-start.22 = (f32[96]{0:T(128)}, f32[96]{0:T(128)S(1)}, u32[]{:S(2)}) copy-start(f32[96]{0:T(128)S(1)} %add_rsqrt_fusion.2) | copy-start | bytes 1156
  28.3 26.9 %copy-start.1 = (bf16[96,2048]{1,0:T(8,128)(2,1)S(1)}, bf16[96,2048]{1,0:T(8,128)(2,1)}, u32[]{:S(2)}) copy-start(bf16[96,2048]{1,0:T(8,128)(2,1)} %param.18) | copy-start | bytes 1179652
  28.4 26.9 %copy-start.21 = (f32[2048]{0:T(1024)S(1)}, f32[2048]{0:T(1024)}, u32[]{:S(2)}) copy-start(f32[2048]{0:T(1024)} %param.25) | copy-start | bytes 24580
  53.7 2.2 %copy-start.17 = (f32[512]{0:T(512)S(1)}, f32[512]{0:T(512)}, u32[]{:S(2)}) copy-start(f32[512]{0:T(512)} %param.29) | copy-start | bytes 6148
  54.0 10.5 %copy-start.6 = (bf16[512,384]{1,0:T(8,128)(2,1)S(1)}, bf16[512,384]{1,0:T(8,128)(2,1)}, u32[]{:S(2)}) copy-start(bf16[512,384]{1,0:T(8,128)(2,1)} %param.31) | copy-start | bytes 1179652
  67.6 0.6 copy-start.11
  70.5 54.6 %copy-start.15 = (f32[384]{0:T(512)S(1)}, f32[384]{0:T(512)}, u32[]{:S(2)}) copy-start(f32[384]{0:T(512)} %get-tuple-element.33) | copy-start | bytes 4612
  70.5 54.6 %copy-start.16 = (f32[384]{0:T(512)S(1)}, f32[384]{0:T(512)}, u32[]{:S(2)}) copy-start(f32[384]{0:T(512)} %get-tuple-element.34) | copy-start | bytes 4612
  81.0 31.9 %copy-start.13 = (bf16[128,64]{0,1:T(8,128)(2,1)S(1)}, bf16[128,64]{0,1:T(8,128)(2,1)}, u32[]{:S(2)}) copy-start(bf16[128,64]{0,1:T(8,128)(2,1)} %param.21) | copy-start | bytes 49156
  81.0 44.1 %copy-start.18 = (f32[16]{0:T(128)S(1)}, f32[16]{0:T(128)}, u32[]{:S(2)}) copy-start(f32[16]{0:T(128)} %multiply_power_fusion) | copy-start | bytes 196
  81.0 44.4 %copy-start.7 = (f32[384,2,16]{0,2,1:T(8,128)S(1)}, f32[384,2,16]{0,2,1:T(8,128)}, u32[]{:S(2)}) copy-start(f32[384,2,16]{0,2,1:T(8,128)} %get-tuple-element.7) | copy-start | bytes 147460
  81.0 44.4 %copy-start.8 = (f32[384,2,16]{0,2,1:T(8,128)S(1)}, f32[384,2,16]{0,2,1:T(8,128)}, u32[]{:S(2)}) copy-start(f32[384,2,16]{0,2,1:T(8,128)} %get-tuple-element.8) | copy-start | bytes 147460
  81.0 44.4 %copy-start.9 = (f32[384,2,16]{0,2,1:T(8,128)S(1)}, f32[384,2,16]{0,2,1:T(8,128)}, u32[]{:S(2)}) copy-start(f32[384,2,16]{0,2,1:T(8,128)} %get-tuple-element.9) | copy-start | bytes 147460
  81.0 44.4 %copy-start.10 = (f32[384,2,16]{0,2,1:T(8,128)S(1)}, f32[384,2,16]{0,2,1:T(8,128)}, u32[]{:S(2)}) copy-start(f32[384,2,16]{0,2,1:T(8,128)} %get-tuple-element.10) | copy-start | bytes 147460
  126.3 1.0 copy-start.20
  143.8 1.0 copy-start.2
where the time goes:
time: 159 us
  blocking collectives  129 us (81%)
  matrix products  18.4 us (12%)
  other arithmetic  7.9 us (5%)
  local copies, waits for them, and re-layouts  3.43 us (2%)
    all_gather x1, blocking collectives, on_device(): lax.all_gather(own_nope, 'sp', axis=0, tiled=True)  16.9 us
    all_gather x1, blocking collectives, on_device(): lax.all_gather(own_values, 'sp', axis=0, tiled=True)  15.6 us
    all_gather x1, blocking collectives, on_device(): lax.all_gather(rope_group, 'sp', axis=0, tiled=True)  14.6 us
    all_gather x1, blocking collectives, on_device(): lax.all_gather(context_latent, 'sp', axis=0, tiled=True)  13.8 us
    psum x1, blocking collectives, on_device(): summed = lax.psum(partials, 'sp')  13.8 us
    all_gather x1, blocking collectives, on_device(): lax.all_gather(context_rope, 'sp', axis=0, tiled=True)  12.2 us
    all_gather x1, blocking collectives, on_device(): lax.all_gather(latent_low, 'tp', axis=0, tiled=True)  8.7 us
    all_gather x1, blocking collectives, on_device(): lax.all_gather(query_low, 'tp', axis=0, tiled=True)  8.53 us

commit v1 on v0

--- a/solution.py
+++ b/solution.py
@@ -10,6 +10,11 @@
 epsilon = 1e-06
 rope_base = 10000.0
 block_limit = 2048
+
+
+def swapped_in(block, axis, along):
+    sent = jnp.stack([block] * lax.axis_size(axis))
+    return jnp.concatenate(lax.all_to_all(sent, axis, 0, 0), axis=along)
 
 
 def rms_scaled(values, gain_vec):
@@ -191,7 +196,7 @@
         (
             lax.all_gather(own_nope, "sp", axis=0, tiled=True),
             lax.all_gather(own_values, "sp", axis=0, tiled=True),
-            lax.all_gather(rope_group, "sp", axis=0, tiled=True),
+            swapped_in(rope_group, "sp", 0),
         ),
         expanded_step,
     )

time: 159 us -> 153 us (0.962)
  blocking collectives: 129 us -> 115 us
  starting transfers between devices: 0 us -> 3.99 us
  matrix products: 18.4 us -> 21.6 us
  other arithmetic: 7.9 us -> 4.7 us
  local copies, waits for them, and re-layouts: 3.43 us -> 6.42 us
    all_gather x1 -> x0, blocking collectives: 14.6 us -> none  [on_device(): lax.all_gather(rope_group, 'sp', axis=0, tiled=True)]
    all_to_all x0 -> x1, starting transfers between devices: none -> 3.99 us  [swapped_in(): return jnp.concatenate(lax.all_to_all(sent, axis, 0, 0), axis=along)]
    all_to_all x0 -> x1, local copies, waits for them, and re-layouts: none -> 1.75 us  [swapped_in(): return jnp.concatenate(lax.all_to_all(sent, axis, 0, 0), axis=along)]
    reshape x0 -> x1, local copies, waits for them, and re-layouts: none -> 1.67 us  [swapped_in(): return jnp.concatenate(lax.all_to_all(sent, axis, 0, 0), axis=along)]
  transfers between devices with their start and end apart: 0 -> 1, of which waited for: 0 -> 0; matrix products, arithmetic and copies ran while one was open for 0% -> 7% of each run, Pallas kernels for 0% -> 0%
where the time goes in v1:
time: 153 us; the launch traced here: 152 us
  blocking collectives  115 us (75%)
  matrix products  21.6 us (14%)
  local copies, waits for them, and re-layouts  6.42 us (4%)
  other arithmetic  4.7 us (3%)
  starting transfers between devices  3.99 us (3%)
    all_gather x1, blocking collectives, on_device(): lax.all_gather(own_values, 'sp', axis=0, tiled=True)  16.5 us
    all_gather x1, blocking collectives, on_device(): lax.all_gather(own_nope, 'sp', axis=0, tiled=True)  16.1 us
    all_gather x1, blocking collectives, on_device(): lax.all_gather(context_latent, 'sp', axis=0, tiled=True)  14.3 us
    psum x1, blocking collectives, on_device(): summed = lax.psum(partials, 'sp')  13.8 us
    all_gather x1, blocking collectives, on_device(): lax.all_gather(context_rope, 'sp', axis=0, tiled=True)  12.2 us
    all_gather x1, blocking collectives, on_device(): lax.all_gather(query_low, 'tp', axis=0, tiled=True)  9.49 us
    all_gather x1, blocking collectives, on_device(): lax.all_gather(rope_keys, 'tp', axis=0, tiled=True)  8.22 us
    all_gather x1, blocking collectives, on_device(): modulation = lax.all_gather(summed, 'tp', axis=1, tiled=True)  8.2 us
  transfers between devices with their start and end apart: 1, of which 0 were waited for; matrix products, arithmetic and copies ran while one was open for 7% of the time, Pallas kernels for 0%

profile of v1, /device:TPU:0, one launch (start us, length us, event | category | flops | bytes accessed | tf_op | source)
XLA Modules:
  0.0 151.7 jit_solution(1987810659149730762)
XLA Ops:
  0.0 0.8 fusion.52
  0.9 1.2 fusion.70
  2.1 1.2 fusion.71
  3.3 1.2 fusion.72
  4.6 13.8 %psum.7 = f32[3,512]{1,0:T(4,128)S(1)} all-reduce(f32[3,512]{1,0:T(4,128)S(1)} %pad_maximum_fusion.2), channel_id=1, replica_groups=mesh['sp'=4,'tp'=4,'dp'=2] {'sp'}, use_global_device_ids=true, to_apply=%region_0.1 | all-reduce | flops 1536 | bytes 12288 | tf_op jit(solution)/shard_map/psum | solution.py:107
  18.3 8.2 %all_gather.24 = f32[3,2048]{1,0:T(4,128)S(1)} all-gather(f32[3,512]{1,0:T(4,128)S(1)} %psum.7), channel_id=1, replica_groups=mesh['sp'=4,'tp'=4,'dp'=2] {'tp'}, dimensions={1}, use_global_device_ids=true | all-gather | bytes 30720 | tf_op jit(solution)/shard_map/all_gather | solution.py:108
  26.6 1.2 fusion.26
  27.8 1.5 fusion.60
  29.5 8.2 %all-gather = bf16[4,96,64]{1,2,0:T(8,128)(2,1)S(1)} all-gather(bf16[1,96,64]{1,2,0:T(8,128)(2,1)S(1)} %fusion.45), channel_id=1, replica_groups=mesh['sp'=4,'tp'=4,'dp'=2] {'tp'}, dimensions={0}, use_global_device_ids=true | all-gather | bytes 61440 | tf_op jit(solution)/shard_map/all_gather | solution.py:132
  37.9 0.7 stack.23
  38.5 4.0 %all-to-all-start = ((bf16[4,384,64]{1,2,0:T(8,128)(2,1)}), bf16[4,384,64]{1,2,0:T(8,128)(2,1)}, u32[]{:S(2)}, u32[]{:S(2)}) async-start(bf16[4,384,64]{1,2,0:T(8,128)(2,1)} %stack.23), calls=%async_computation | async-start | bytes 393216 | tf_op jit(solution)/shard_map/all_to_all | solution.py:17
  42.6 1.7 %multiply_reduce_fusion.1 = (f32[96]{0:T(128)S(1)}, f32[96,256]{1,0:T(8,128)S(1)}) fusion(bf16[2048,256]{1,0:T(8,128)(2,1)} %param.27, bf16[96,2048]{1,0:T(8,128)(2,1)S(1)} %copy-done.3, f32[2048]{0:T(1024)S(1)} %bitcast.120, f32[2048]{0:T(1024)S(1)} %bitcast.123, f32[2048]{0:T(1024)S(1)} %copy-done.20, f32[96]{0:T(128)S(1)} %add_rsqrt_fusion.2), kind=kOutput, calls=%fused_computation.48 | convolution fusion | flops 101892000 | bytes 1565440 | tf_op jit(solution)/shard_map/dot_general | solution.py:120
  44.4 7.7 %all_gather.28 = bf16[384,256]{1,0:T(8,128)(2,1)S(1)} all-gather(bf16[96,256]{1,0:T(8,128)(2,1)S(1)} %multiply_convert_fusion.1), channel_id=1, replica_groups=mesh['sp'=4,'tp'=4,'dp'=2] {'tp'}, dimensions={0}, use_global_device_ids=true | all-gather | bytes 245760 | tf_op jit(solution)/shard_map/all_gather | solution.py:131
  52.1 14.3 %all_gather.26 = bf16[512,256]{1,0:T(8,128)(2,1)S(1)} all-gather(bf16[128,256]{1,0:T(8,128)(2,1)S(1)} %copy-done.15), channel_id=1, replica_groups=mesh['sp'=4,'tp'=4,'dp'=2] {'sp'}, dimensions={0}, use_global_device_ids=true | all-gather | bytes 327680 | tf_op jit(solution)/shard_map/all_gather | solution.py:146
  66.4 0.9 convolution_convert_fusion.3
  67.3 1.0 convolution_convert_fusion.1
  68.3 1.0 convolution_convert_fusion
  69.2 0.9 convolution_convert_fusion.2
  70.9 9.5 %all_gather.25 = bf16[384,512]{1,0:T(8,128)(2,1)S(1)} all-gather(bf16[96,512]{1,0:T(8,128)(2,1)S(1)} %multiply_convert_fusion), channel_id=1, replica_groups=mesh['sp'=4,'tp'=4,'dp'=2] {'tp'}, dimensions={0}, use_global_device_ids=true | all-gather | bytes 491520 | tf_op jit(solution)/shard_map/all_gather | solution.py:130
  81.5 16.1 %all_gather.29 = bf16[1536,256]{1,0:T(8,128)(2,1)S(1)} all-gather(bf16[384,256]{1,0:T(8,128)(2,1)} %convolution_convert_fusion.3), channel_id=1, replica_groups=mesh['sp'=4,'tp'=4,'dp'=2] {'sp'}, dimensions={0}, use_global_device_ids=true | all-gather | bytes 983040 | tf_op jit(solution)/shard_map/all_gather | solution.py:197
  97.6 1.4 fusion.41
  99.0 12.2 %all_gather.27 = bf16[512,64]{0,1:T(8,128)(2,1)S(1)} all-gather(bf16[128,64]{0,1:T(8,128)(2,1)S(1)} %copy-done.16), channel_id=1, replica_groups=mesh['sp'=4,'tp'=4,'dp'=2] {'sp'}, dimensions={0}, use_global_device_ids=true | all-gather | bytes 81920 | tf_op jit(solution)/shard_map/all_gather | solution.py:147
  112.1 1.2 copy-done.1
  113.7 16.5 %all_gather.31 = bf16[1536,256]{1,0:T(8,128)(2,1)} all-gather(bf16[384,256]{1,0:T(8,128)(2,1)S(1)} %copy-done.8), channel_id=1, replica_groups=mesh['sp'=4,'tp'=4,'dp'=2] {'sp'}, dimensions={0}, use_global_device_ids=true | all-gather | bytes 983040 | tf_op jit(solution)/shard_map/all_gather | solution.py:198
  130.2 1.7 %copy.50 = bf16[4,384,64]{1,0,2:T(4,128)(2,1)} copy(bf16[4,384,64]{1,2,0:T(8,128)(2,1)} %all-to-all-done) | data formatting | bytes 393216 | tf_op jit(solution)/shard_map/all_to_all | solution.py:17
  131.9 1.7 %reshape.268 = bf16[1536,64,1]{0,1,2:T(8,128)(2,1)} reshape(bf16[4,384,64]{1,0,2:T(4,128)(2,1)} %copy.50) | data formatting | bytes 393216 | tf_op jit(solution)/shard_map/reshape | solution.py:17
  133.6 1.8 %fusion.74 = f32[1536,384,2]{0,1,2:T(8,128)S(1)} fusion(bf16[1536,64,1]{0,1,2:T(8,128)(2,1)} %reshape.268, bf16[384,2,64]{0,2,1:T(8,128)(2,1)} %copy-done.6), kind=kOutput, calls=%fused_computation.115 | convolution fusion | flops 150994944 | bytes 5013504 | tf_op jit(solution)/shard_map/thr,kr->htk/dot_general | solution.py:45
  135.4 1.0 fusion.69
  136.5 0.8 fusion.1
  138.6 0.9 fusion.23
  139.8 8.1 %all_to_all.24 = bf16[4,96,256]{2,1,0:T(8,128)(2,1)S(1)} all-to-all(bf16[4,96,256]{2,1,0:T(8,128)(2,1)S(1)} %all_to_all.18), channel_id=1, replica_groups=mesh['sp'=4,'tp'=4,'dp'=2] {'tp'}, dimensions={0} | all-to-all | bytes 393216 | tf_op jit(solution)/shard_map/all_to_all | solution.py:205
  147.9 3.8 %fusion.7 = bf16[96,2048]{1,0:T(8,128)(2,1)} fusion(bf16[96,1024]{1,0:T(8,128)(2,1)S(1)} %bitcast.116, bf16[1024,2048]{1,0:T(8,128)(2,1)} %param.35, bf16[96,2048]{1,0:T(8,128)(2,1)S(1)} %copy-done.4, f32[2048]{0:T(1024)S(1)} %bitcast.118), kind=kOutput, calls=%fused_computation.9 | convolution fusion | flops 403439616 | bytes 5185536 | tf_op jit(solution)/shard_map/dot_general | solution.py:206
  (72 shorter events, 5.2 us)
Async XLA Ops:
  0.0 70.1 %copy-start = (bf16[2048,512]{1,0:T(8,128)(2,1)S(1)}, bf16[2048,512]{1,0:T(8,128)(2,1)}, u32[]{:S(2)}) copy-start(bf16[2048,512]{1,0:T(8,128)(2,1)} %param.26) | copy-start | bytes 6291460
  0.0 42.5 %copy-start.3 = (bf16[96,2048]{1,0:T(8,128)(2,1)S(1)}, bf16[96,2048]{1,0:T(8,128)(2,1)}, u32[]{:S(2)}) copy-start(bf16[96,2048]{1,0:T(8,128)(2,1)} %param.18) | copy-start | bytes 1179652
  0.0 42.5 %copy-start.20 = (f32[2048]{0:T(1024)S(1)}, f32[2048]{0:T(1024)}, u32[]{:S(2)}) copy-start(f32[2048]{0:T(1024)} %param.25) | copy-start | bytes 24580
  26.5 17.7 %copy-start.18 = (f32[256]{0:T(256)S(1)}, f32[256]{0:T(256)}, u32[]{:S(2)}) copy-start(f32[256]{0:T(256)} %param.30) | copy-start | bytes 3076
  27.8 24.3 %copy-start.15 = (bf16[128,256]{1,0:T(8,128)(2,1)S(1)}, bf16[128,256]{1,0:T(8,128)(2,1)}, u32[]{:S(2)}) copy-start(bf16[128,256]{1,0:T(8,128)(2,1)} %param.20) | copy-start | bytes 196612
  27.8 38.6 %copy-start.9 = (bf16[256,256]{1,0:T(8,128)(2,1)S(1)}, bf16[256,256]{1,0:T(8,128)(2,1)}, u32[]{:S(2)}) copy-start(bf16[256,256]{1,0:T(8,128)(2,1)} %param.32) | copy-start | bytes 393220
  37.7 30.6 %copy-start.10 = (bf16[256,256]{1,0:T(8,128)(2,1)S(1)}, bf16[256,256]{1,0:T(8,128)(2,1)}, u32[]{:S(2)}) copy-start(bf16[256,256]{1,0:T(8,128)(2,1)} %param.33) | copy-start | bytes 393220
  38.5 91.6 %all-to-all-start = ((bf16[4,384,64]{1,2,0:T(8,128)(2,1)}), bf16[4,384,64]{1,2,0:T(8,128)(2,1)}, u32[]{:S(2)}, u32[]{:S(2)}) async-start(bf16[4,384,64]{1,2,0:T(8,128)(2,1)} %stack.23), calls=%async_computation | async-start | bytes 393216 | tf_op jit(solution)/shard_map/all_to_all | solution.py:17
  67.3 3.5 %copy-start.17 = (f32[512]{0:T(512)S(1)}, f32[512]{0:T(512)}, u32[]{:S(2)}) copy-start(f32[512]{0:T(512)} %param.29) | copy-start | bytes 6148
  68.3 12.1 %copy-start.11 = (bf16[512,384]{1,0:T(8,128)(2,1)S(1)}, bf16[512,384]{1,0:T(8,128)(2,1)}, u32[]{:S(2)}) copy-start(bf16[512,384]{1,0:T(8,128)(2,1)} %param.31) | copy-start | bytes 1179652
  80.3 18.6 %copy-start.16 = (bf16[128,64]{0,1:T(8,128)(2,1)S(1)}, bf16[128,64]{0,1:T(8,128)(2,1)}, u32[]{:S(2)}) copy-start(bf16[128,64]{0,1:T(8,128)(2,1)} %param.21) | copy-start | bytes 49156
  80.8 30.8 %copy-start.19 = (f32[2]{0:T(128)S(1)}, f32[2]{0:T(128)}, u32[]{:S(2)}) copy-start(f32[2]{0:T(128)} %param.34) | copy-start | bytes 28
  81.5 30.0 %copy-start.12 = (f32[384,2,16]{0,2,1:T(8,128)S(1)}, f32[384,2,16]{0,2,1:T(8,128)}, u32[]{:S(2)}) copy-start(f32[384,2,16]{0,2,1:T(8,128)} %get-tuple-element.8) | copy-start | bytes 147460
  81.5 30.0 %copy-start.13 = (f32[384,2,16]{0,2,1:T(8,128)S(1)}, f32[384,2,16]{0,2,1:T(8,128)}, u32[]{:S(2)}) copy-start(f32[384,2,16]{0,2,1:T(8,128)} %get-tuple-element.9) | copy-start | bytes 147460
  81.5 30.0 %copy-start.14 = (f32[384,2,16]{0,2,1:T(8,128)S(1)}, f32[384,2,16]{0,2,1:T(8,128)}, u32[]{:S(2)}) copy-start(f32[384,2,16]{0,2,1:T(8,128)} %get-tuple-element.10) | copy-start | bytes 147460
  111.6 2.1 %copy-start.6 = (bf16[384,2,64]{0,2,1:T(8,128)(2,1)}, bf16[384,2,64]{0,2,1:T(8,128)(2,1)S(1)}, u32[]{:S(2)}) copy-start(bf16[384,2,64]{0,2,1:T(8,128)(2,1)S(1)} %fusion.38) | copy-start | bytes 294916
  111.6 2.1 %copy-start.8 = (bf16[384,256]{1,0:T(8,128)(2,1)S(1)}, bf16[384,256]{1,0:T(8,128)(2,1)}, u32[]{:S(2)}) copy-start(bf16[384,256]{1,0:T(8,128)(2,1)} %convolution_convert_fusion.2) | copy-start | bytes 589828
  112.1 1.2 copy-start.1
  136.4 1.4 copy-start.2
  136.4 1.4 copy-start.5
  136.4 2.1 %copy-start.7 = (bf16[1536,256]{1,0:T(8,128)(2,1)S(1)}, bf16[1536,256]{1,0:T(8,128)(2,1)}, u32[]{:S(2)}) copy-start(bf16[1536,256]{1,0:T(8,128)(2,1)} %all_gather.31) | copy-start | bytes 2359300
  138.5 9.4 %copy-start.4 = (bf16[96,2048]{1,0:T(8,128)(2,1)S(1)}, bf16[96,2048]{1,0:T(8,128)(2,1)}, u32[]{:S(2)}) copy-start(bf16[96,2048]{1,0:T(8,128)(2,1)} %param.18) | copy-start | bytes 1179652
